TPU v7x, 128 devices: a whole 4x4x4 slice. The times are simulated.
128 devices in a mesh: sp: 32 (over z, y, core), tp: 4 (over x).
Axes of the slice: x: 4, y: 4, z: 4, core: 2. Of those that a mesh axis runs over, the one named last changes fastest.
Arguments:
- queries: bfloat16 [32768, 1024], P('sp', 'tp'), may hold values from -8 to 8
- keys: bfloat16 [32768, 256], P('sp', 'tp'), may hold values from -8 to 8
- values: bfloat16 [32768, 256], P('sp', 'tp'), may hold values from -18 to 18
- doc_ids: int32 [32768], P('sp'), may hold values from 0 to 7, never falling along the last dimension, each value on 1 to 16384 neighbouring positions
- sinks: float32 [16], P('tp'), may hold values from 0 to 4
- residual: bfloat16 [32768, 2048], P(('sp', 'tp')), may hold values from -12 to 12
- out_weight: bfloat16 [1024, 2048], P('tp'), may hold values from -0.1875 to 0.1875
- norm_gain: float32 [2048], replicated, may hold values from 0.1 to 1.9
- w_gate: bfloat16 [2048, 5632], P('sp', 'tp'), may hold values from -0.125 to 0.125
- w_value: bfloat16 [2048, 5632], P('sp', 'tp'), may hold values from -0.125 to 0.125
- conv_gate: float32 [3, 5632], P(None, 'tp'), may hold values from -3.5 to 3.5
- conv_value: float32 [3, 5632], P(None, 'tp'), may hold values from -3.5 to 3.5
- w_down: bfloat16 [5632, 2048], P('tp', 'sp'), may hold values from -0.078125 to 0.078125
Outputs:
- layer_out: bfloat16 [32768, 2048], P(('sp', 'tp'))
All inputs are finite; a program needn't handle non-finite values.
Results may differ from a plain program's by a relative error of at most 0.012.
Values may be sent and summed in bfloat16 or wider, within the bound.
A program may use at most 128 MiB of HBM per device.

v0:
```python
import jax
import jax.numpy as jnp
from jax import lax
from jax.sharding import PartitionSpec as P

HEAD_DIM = 64
WINDOW = 128


def shifted(shard, axis, by):
    size = lax.axis_size(axis)
    pairs = [(i, i + by) for i in range(size) if 0 <= i + by < size]
    return lax.ppermute(shard, axis, pairs)


def joined_along(pieces, dim):
    shape = list(pieces.shape[1:])
    shape[dim] *= pieces.shape[0]
    return jnp.moveaxis(pieces, 0, dim).reshape(shape)


def sent_to_all(shard, axis):
    size = lax.axis_size(axis)
    return lax.all_to_all(
        jnp.broadcast_to(shard[None], (size, *shard.shape)), axis, 0, 0, tiled=True
    )


def gathered_copies(shard, axis, dim):
    return joined_along(sent_to_all(shard, axis), dim)


def side_by_side(arrays, axis, dim, along):
    both = jnp.concatenate(arrays, axis=along)
    out, at, done = (lax.all_gather(both, axis, axis=dim, tiled=True), 0, [])
    for a in arrays:
        done.append(lax.slice_in_dim(out, at, at + a.shape[along], axis=along))
        at += a.shape[along]
    return tuple(done)


def attend(query_rows, key_ext, value_ext, doc_rows, doc_ext, sinks):
    row_count = query_rows.shape[0]
    block_count = row_count // WINDOW
    kv_heads = key_ext.shape[1] // HEAD_DIM
    group_size = query_rows.shape[1] // (kv_heads * HEAD_DIM)

    def band(t):
        lower = t[:row_count].reshape((block_count, WINDOW) + t.shape[1:])
        upper = t[WINDOW:].reshape((block_count, WINDOW) + t.shape[1:])
        return jnp.concatenate([lower, upper], axis=1)

    query_band = query_rows.reshape(block_count, WINDOW, kv_heads, group_size, HEAD_DIM)
    key_band = band(key_ext).reshape(block_count, 2 * WINDOW, kv_heads, HEAD_DIM)
    value_band = band(value_ext).reshape(block_count, 2 * WINDOW, kv_heads, HEAD_DIM)
    doc_band = band(doc_ext)
    distance = jnp.arange(WINDOW)[:, None] + WINDOW - jnp.arange(2 * WINDOW)[None, :]
    in_window = (distance >= 0) & (distance < WINDOW)
    same_doc = doc_rows.reshape(block_count, WINDOW)[:, :, None] == doc_band[:, None, :]
    keep_mask = in_window[None] & same_doc
    scores = jnp.einsum(
        "nqhgd,nkhd->nhgqk", query_band, key_band, preferred_element_type=jnp.float32
    ) * HEAD_DIM ** (-0.5)
    scores = jnp.where(keep_mask[:, None, None], scores, -jnp.inf)
    sink_logit = sinks.reshape(kv_heads, group_size)[None, :, :, None, None]
    peak = jnp.maximum(jnp.max(scores, axis=-1, keepdims=True), sink_logit)
    expd = jnp.exp(scores - peak)
    probs = (expd / (jnp.sum(expd, axis=-1, keepdims=True) + jnp.exp(sink_logit - peak))).astype(
        jnp.bfloat16
    )
    mixed = jnp.einsum("nhgqk,nkhd->nqhgd", probs, value_band, preferred_element_type=jnp.float32)
    return mixed.astype(jnp.bfloat16).reshape(row_count, -1)


def convolve(ext_rows, doc_ext, taps):
    center = doc_ext[2:]
    same_one = (doc_ext[1:-1] == center)[:, None]
    same_two = (doc_ext[:-2] == center)[:, None]
    ext32 = ext_rows.astype(jnp.float32)
    result = taps[2] * ext32[2:]
    result = result + jnp.where(same_one, taps[1] * ext32[1:-1], 0.0)
    return result + jnp.where(same_two, taps[0] * ext32[:-2], 0.0)


def per_device(
    queries,
    keys,
    values,
    doc_ids,
    sinks,
    residual,
    out_weight,
    norm_gain,
    w_gate,
    w_value,
    conv_gate,
    conv_value,
    w_down,
):
    docs_plus = doc_ids + 1
    prev_keys, prev_values, prev_docs = shifted(
        (keys[-WINDOW:], values[-WINDOW:], docs_plus[-WINDOW:]), "sp", 1
    )
    key_ext = jnp.concatenate([prev_keys, keys], axis=0)
    value_ext = jnp.concatenate([prev_values, values], axis=0)
    doc_ext = jnp.concatenate([prev_docs, docs_plus], axis=0)
    head_out = attend(queries, key_ext, value_ext, docs_plus, doc_ext, sinks)
    head_rows = lax.all_to_all(head_out, "tp", split_axis=0, concat_axis=1, tiled=True)
    proj = jnp.dot(
        head_rows,
        lax.all_gather(out_weight, "tp", axis=0, tiled=True),
        preferred_element_type=jnp.float32,
    )
    mid32 = (residual.astype(jnp.float32) + proj).astype(jnp.bfloat16).astype(jnp.float32)
    normed = (
        mid32 * lax.rsqrt(jnp.mean(mid32 * mid32, axis=-1, keepdims=True) + 1e-06) * norm_gain
    ).astype(jnp.bfloat16)
    whole = gathered_copies(normed, "tp", 0)

    def add_rows(piece):
        return jnp.dot(whole, piece, preferred_element_type=jnp.float32)

    pieces = side_by_side((w_gate, w_value), "sp", 0, 1)
    gate_sum = add_rows(pieces[0])
    value_sum = add_rows(pieces[1])
    gate_pre = gate_sum.astype(jnp.bfloat16)
    value_pre = value_sum.astype(jnp.bfloat16)
    prev_gate, prev_value = shifted((gate_pre[-2:], value_pre[-2:]), "sp", 1)
    conv_docs = jnp.concatenate([prev_docs[-2:], docs_plus], axis=0)
    gate_conv = convolve(jnp.concatenate([prev_gate, gate_pre], axis=0), conv_docs, conv_gate)
    value_conv = convolve(jnp.concatenate([prev_value, value_pre], axis=0), conv_docs, conv_value)
    hidden = (jax.nn.silu(gate_conv) * value_conv).astype(jnp.bfloat16)
    terms = jnp.dot(
        hidden, lax.all_gather(w_down, "sp", axis=1, tiled=True), preferred_element_type=jnp.float32
    )
    sums = lax.psum_scatter(
        terms.astype(jnp.bfloat16), "tp", scatter_dimension=0, tiled=True
    ).astype(jnp.float32)
    return (mid32 + sums).astype(jnp.bfloat16)


def solution(mesh):
    return jax.shard_map(
        per_device,
        mesh=mesh,
        in_specs=(
            P("sp", "tp"),
            P("sp", "tp"),
            P("sp", "tp"),
            P("sp"),
            P("tp"),
            P(("sp", "tp"), None),
            P("tp", None),
            P(),
            P("sp", "tp"),
            P("sp", "tp"),
            P(None, "tp"),
            P(None, "tp"),
            P("tp", "sp"),
        ),
        out_specs=P(("sp", "tp"), None),
        check_vma=False,
    )
```

profile of v0, /device:TPU:1, one launch (start us, length us, event | category | flops | bytes accessed | tf_op | source)
XLA Modules:
  0.0 256.3 jit_solution(1870494783780439739)
XLA Ops:
  7.3 1.8 pad_maximum_fusion
  9.8 4.6 %collective-permute-start.1 = (s32[128]{0:T(128)S(1)}, s32[128]{0:T(128)S(1)}, u32[]{:S(2)}, u32[]{:S(2)}) collective-permute-start(s32[128]{0:T(128)S(1)} %slice.89), channel_id=1, source_target_pairs={{0,4},{4,8},{8,12},{12,16},{16,20},{20,24},{24,28},{28,32},{32,36}... | collective-permute-start | bytes 1544 | tf_op jit(solution)/shard_map/ppermute | solution.py:13
  15.2 1.9 collective-permute-start.2
  17.8 3.6 %collective-permute-start = (bf16[128,64]{0,1:T(8,128)(2,1)S(1)}, bf16[128,64]{0,1:T(8,128)(2,1)S(1)}, u32[]{:S(2)}, u32[]{:S(2)}) collective-permute-start(bf16[128,64]{0,1:T(8,128)(2,1)S(1)} %slice.87), channel_id=1, source_target_pairs={{0,4},{4,8},{8,12},{12,16},{16,20},{20,24},{24,28},{28,32},{32,36}... | collective-permute-start | bytes 49160 | tf_op jit(solution)/shard_map/ppermute | solution.py:13
  23.4 2.1 reshape.131
  26.9 1.0 fusion.20
  28.0 1.2 fusion.34
  30.0 19.1 %all_to_all.24 = bf16[4,256,256]{1,2,0:T(8,128)(2,1)S(1)} all-to-all(bf16[4,256,256]{1,2,0:T(8,128)(2,1)S(1)} %copy.33), channel_id=1, replica_groups=mesh['sp'=32,'tp'=4] {'tp'}, dimensions={0} | all-to-all | bytes 1048576 | tf_op jit(solution)/shard_map/all_to_all | solution.py:108
  49.1 16.7 %all-gather.4.cloned.1.call-done = bf16[1024,2048]{1,0:T(8,128)(2,1)} async-done(((bf16[256,2048]{1,0:T(8,128)(2,1)}), bf16[1024,2048]{1,0:T(8,128)(2,1)}) %all-gather.4.cloned.1.call-update) | async-done | bytes 4194320 | tf_op jit(solution)/shard_map/all_gather | solution.py:111
  65.8 3.6 %fusion.24 = (f32[256]{0:T(256)S(1)}, bf16[256,2048]{1,0:T(8,128)(2,1)S(1)}) fusion(bf16[256,1024]{0,1:T(8,128)(2,1)S(1)} %bitcast.77, bf16[1024,2048]{1,0:T(8,128)(2,1)} %all-gather.4.cloned.1.call-done, bf16[256,2048]{1,0:T(8,128)(2,1)S(1)} %copy-done.7), kind=kOutput, calls=%fused_computation.35 | convolution fusion | flops 1076887296 | bytes 6816768 | tf_op jit(solution)/shard_map/dot_general | solution.py:109
  69.8 2.6 broadcast_in_dim.59
  72.3 5.0 %all-to-all-start.1 = ((bf16[4,256,2048]{2,1,0:T(8,128)(2,1)}), bf16[4,256,2048]{2,1,0:T(8,128)(2,1)}, u32[]{:S(2)}, u32[]{:S(2)}) async-start(bf16[4,256,2048]{2,1,0:T(8,128)(2,1)} %broadcast_in_dim.59), calls=%async_computation.1 | async-start | bytes 8388608 | tf_op jit(solution)/shard_map/all_to_all | solution.py:24
  77.7 47.8 %all-to-all-done.1 = bf16[4,256,2048]{2,1,0:T(8,128)(2,1)} async-done(((bf16[4,256,2048]{2,1,0:T(8,128)(2,1)}), bf16[4,256,2048]{2,1,0:T(8,128)(2,1)}, u32[]{:S(2)}, u32[]{:S(2)}) %all-to-all-start.1) | async-done | bytes 4194336 | tf_op jit(solution)/shard_map/all_to_all | solution.py:24
  125.5 3.9 %all-gather.6.cloned.1.call-done = bf16[2048,2816]{1,0:T(8,128)(2,1)} async-done(((bf16[64,2816]{1,0:T(8,128)(2,1)}), bf16[2048,2816]{1,0:T(8,128)(2,1)}) %all-gather.6.cloned.1.call-update) | async-done | bytes 11534352 | tf_op jit(solution)/shard_map/all_gather | solution.py:35
  129.3 10.3 %fusion.14 = bf16[1024,1408]{1,0:T(8,128)(2,1)S(1)} fusion(bf16[1024,2048]{1,0:T(8,128)(2,1)} %bitcast.13, bf16[2048,2816]{1,0:T(8,128)(2,1)} %all-gather.6.cloned.1.call-done), kind=kOutput, calls=%fused_computation.23 | convolution fusion | flops 5907021824 | bytes 12845056 | tf_op jit(solution)/shard_map/dot_general | solution.py:121
  139.6 3.4 %collective-permute-start.3 = (bf16[2,1408]{1,0:T(2,128)(2,1)S(1)}, bf16[2,1408]{1,0:T(2,128)(2,1)S(1)}, u32[]{:S(2)}, u32[]{:S(2)}) collective-permute-start(bf16[2,1408]{1,0:T(2,128)(2,1)S(1)} %slice.114), channel_id=1, source_target_pairs={{0,4},{4,8},{8,12},{12,16},{16,20},{20,24},{24,28},{28,32},{32,36}... | collective-permute-start | bytes 16904 | tf_op jit(solution)/shard_map/ppermute | solution.py:13
  143.1 8.5 %fusion.17 = bf16[1024,1408]{1,0:T(8,128)(2,1)S(1)} fusion(bf16[1024,2048]{1,0:T(8,128)(2,1)} %bitcast.13, bf16[2048,2816]{1,0:T(8,128)(2,1)S(1)} %copy-done.6), kind=kOutput, calls=%fused_computation.24 | convolution fusion | flops 5907021824 | bytes 12845056 | tf_op jit(solution)/shard_map/dot_general | solution.py:121
  151.6 2.2 collective-permute-start.4
  153.8 3.0 %maximum_convert_fusion = f32[1026,1408]{1,0:T(8,128)} fusion(bf16[1024,1408]{1,0:T(8,128)(2,1)S(1)} %fusion.14, bf16[2,1408]{1,0:T(2,128)(2,1)S(1)} %collective-permute-done.3), kind=kLoop, calls=%fused_computation.31 | loop fusion | flops 5778432 | bytes 8667648 | tf_op jit(solution)/shard_map/convert_element_type | solution.py:79
  156.8 3.1 %maximum_convert_fusion.1 = f32[1026,1408]{1,0:T(8,128)} fusion(bf16[1024,1408]{1,0:T(8,128)(2,1)S(1)} %fusion.17, bf16[2,1408]{1,0:T(2,128)(2,1)S(1)} %collective-permute-done.4), kind=kLoop, calls=%fused_computation.32 | loop fusion | flops 5778432 | bytes 8667648 | tf_op jit(solution)/shard_map/convert_element_type | solution.py:79
  159.9 19.4 %all-gather.8.cloned.1.call-done = bf16[1408,2048]{0,1:T(8,128)(2,1)} async-done(((bf16[1408,64]{0,1:T(8,128)(2,1)}), bf16[1408,2048]{0,1:T(8,128)(2,1)}) %all-gather.8.cloned.1.call-update) | async-done | bytes 5767184 | tf_op jit(solution)/shard_map/all_gather | solution.py:134
  179.3 22.3 %convolution_convert_fusion = bf16[1024,2048]{1,0:T(8,128)(2,1)} fusion(bf16[1408,2048]{0,1:T(8,128)(2,1)} %all-gather.8.cloned.1.call-done, f32[1026,1408]{1,0:T(8,128)} %maximum_convert_fusion.1, f32[1026,1408]{1,0:T(8,128)} %maximum_convert_fusion, f32[1408]{0:T(1024)S(1)} %get-tuple-element.9, f32[1408]{0:T(1024)S(1)} %get-tuple-element.10, ...), kind=kOutput, calls=%fused_computation.25 | convolution fusion | flops 5936513024 | bytes 44600320 | tf_op jit(solution)/shard_map/dot_general | solution.py:133
  201.7 45.4 %reduce-scatter.2.cloned.1.call-done = bf16[256,2048]{1,0:T(8,128)(2,1)} async-done(((bf16[1024,2048]{1,0:T(8,128)(2,1)}), bf16[256,2048]{1,0:T(8,128)(2,1)}) %reduce-scatter.2.cloned.1.call-update) | async-done | bytes 1048592 | tf_op jit(solution)/shard_map/reduce_scatter | solution.py:136
  247.1 2.6 %fusion.27 = bf16[256,2048]{1,0:T(8,128)(2,1)} fusion(bf16[256,2048]{1,0:T(8,128)(2,1)S(1)} %get-tuple-element.18, bf16[256,2048]{1,0:T(8,128)(2,1)} %reduce-scatter.2.cloned.1.call-done), kind=kLoop, calls=%fused_computation.38 | loop fusion | flops 2097152 | bytes 3145728 | tf_op jit(solution)/shard_map/convert_element_type | solution.py:139
  (55 shorter events, 7.8 us)
Async XLA Ops:
  6.5 19.3 %copy-start = (bf16[1024,64]{0,1:T(8,128)(2,1)S(1)}, bf16[1024,64]{0,1:T(8,128)(2,1)}, u32[]{:S(2)}) copy-start(bf16[1024,64]{0,1:T(8,128)(2,1)} %param.14) | copy-start | bytes 393220
  6.5 59.3 %all-gather.4.cloned.1.call-start = ((), (), s32[]{:S(2)}) async-start(), calls=%async_computation.3 | async-start | bytes 5242880 | tf_op jit(solution)/shard_map/all_gather | solution.py:111
  7.3 122.1 %all-gather.6.cloned.1.call-start = ((), (), s32[]{:S(2)}) async-start(), calls=%async_computation.4 | async-start | bytes 11894784 | tf_op jit(solution)/shard_map/all_gather | solution.py:35
  9.1 170.2 %all-gather.8.cloned.1.call-start = ((), (), s32[]{:S(2)}) async-start(), calls=%async_computation.5 | async-start | bytes 5947392 | tf_op jit(solution)/shard_map/all_gather | solution.py:134
  9.8 15.6 %collective-permute-start.1 = (s32[128]{0:T(128)S(1)}, s32[128]{0:T(128)S(1)}, u32[]{:S(2)}, u32[]{:S(2)}) collective-permute-start(s32[128]{0:T(128)S(1)} %slice.89), channel_id=1, source_target_pairs={{0,4},{4,8},{8,12},{12,16},{16,20},{20,24},{24,28},{28,32},{32,36}... | collective-permute-start | bytes 1544 | tf_op jit(solution)/shard_map/ppermute | solution.py:13
  15.2 10.7 %collective-permute-start.2 = (bf16[128,64]{0,1:T(8,128)(2,1)S(1)}, bf16[128,64]{0,1:T(8,128)(2,1)S(1)}, u32[]{:S(2)}, u32[]{:S(2)}) collective-permute-start(bf16[128,64]{0,1:T(8,128)(2,1)S(1)} %slice.92), channel_id=1, source_target_pairs={{0,4},{4,8},{8,12},{12,16},{16,20},{20,24},{24,28},{28,32},{32,36}... | collective-permute-start | bytes 49160 | tf_op jit(solution)/shard_map/ppermute | solution.py:13
  17.8 10.2 %collective-permute-start = (bf16[128,64]{0,1:T(8,128)(2,1)S(1)}, bf16[128,64]{0,1:T(8,128)(2,1)S(1)}, u32[]{:S(2)}, u32[]{:S(2)}) collective-permute-start(bf16[128,64]{0,1:T(8,128)(2,1)S(1)} %slice.87), channel_id=1, source_target_pairs={{0,4},{4,8},{8,12},{12,16},{16,20},{20,24},{24,28},{28,32},{32,36}... | collective-permute-start | bytes 49160 | tf_op jit(solution)/shard_map/ppermute | solution.py:13
  22.4 4.5 %copy-start.5 = (f32[4]{0:T(128)S(1)}, f32[4]{0:T(128)}, u32[]{:S(2)}) copy-start(f32[4]{0:T(128)} %param.17) | copy-start | bytes 52
  25.9 2.1 copy-start.1
  29.2 36.6 %copy-start.7 = (bf16[256,2048]{1,0:T(8,128)(2,1)S(1)}, bf16[256,2048]{1,0:T(8,128)(2,1)}, u32[]{:S(2)}) copy-start(bf16[256,2048]{1,0:T(8,128)(2,1)} %param.18) | copy-start | bytes 3145732
  49.1 20.3 %copy-start.4 = (f32[2048]{0:T(1024)S(1)}, f32[2048]{0:T(1024)}, u32[]{:S(2)}) copy-start(f32[2048]{0:T(1024)} %param.20) | copy-start | bytes 24580
  72.3 5.0 %copy-start.2 = (f32[3,1408]{1,0:T(4,128)S(1)}, f32[3,1408]{1,0:T(4,128)}, u32[]{:S(2)}) copy-start(f32[3,1408]{1,0:T(4,128)} %param.24) | copy-start | bytes 50692
  72.3 5.1 %copy-start.3 = (f32[3,1408]{1,0:T(4,128)S(1)}, f32[3,1408]{1,0:T(4,128)}, u32[]{:S(2)}) copy-start(f32[3,1408]{1,0:T(4,128)} %param.23) | copy-start | bytes 50692
  72.3 53.1 %all-to-all-start.1 = ((bf16[4,256,2048]{2,1,0:T(8,128)(2,1)}), bf16[4,256,2048]{2,1,0:T(8,128)(2,1)}, u32[]{:S(2)}, u32[]{:S(2)}) async-start(bf16[4,256,2048]{2,1,0:T(8,128)(2,1)} %broadcast_in_dim.59), calls=%async_computation.1 | async-start | bytes 8388608 | tf_op jit(solution)/shard_map/all_to_all | solution.py:24
  77.3 169.8 %reduce-scatter.2.cloned.1.call-start = ((), (), s32[]{:S(2)}) async-start(), calls=%async_computation.6 | async-start | bytes 5242880 | tf_op jit(solution)/shard_map/reduce_scatter | solution.py:136
  129.3 13.7 %copy-start.6 = (bf16[2048,2816]{1,0:T(8,128)(2,1)S(1)}, bf16[2048,2816]{1,0:T(8,128)(2,1)}, u32[]{:S(2)}) copy-start(bf16[2048,2816]{1,0:T(8,128)(2,1)} %all-gather.6.cloned.1.call-done) | copy-start | bytes 34603012
  139.6 14.1 %collective-permute-start.3 = (bf16[2,1408]{1,0:T(2,128)(2,1)S(1)}, bf16[2,1408]{1,0:T(2,128)(2,1)S(1)}, u32[]{:S(2)}, u32[]{:S(2)}) collective-permute-start(bf16[2,1408]{1,0:T(2,128)(2,1)S(1)} %slice.114), channel_id=1, source_target_pairs={{0,4},{4,8},{8,12},{12,16},{16,20},{20,24},{24,28},{28,32},{32,36}... | collective-permute-start | bytes 16904 | tf_op jit(solution)/shard_map/ppermute | solution.py:13
  151.6 5.2 %collective-permute-start.4 = (bf16[2,1408]{1,0:T(2,128)(2,1)S(1)}, bf16[2,1408]{1,0:T(2,128)(2,1)S(1)}, u32[]{:S(2)}, u32[]{:S(2)}) collective-permute-start(bf16[2,1408]{1,0:T(2,128)(2,1)S(1)} %slice.121), channel_id=1, source_target_pairs={{0,4},{4,8},{8,12},{12,16},{16,20},{20,24},{24,28},{28,32},{32,36}... | collective-permute-start | bytes 16904 | tf_op jit(solution)/shard_map/ppermute | solution.py:13
Sparse Core Ops, SparseCore 0:
  9.0 56.8 all-gather.3
  68.1 61.1 all-gather.5
  131.6 47.7 all-gather.7
  201.8 45.2 reduce-scatter.1
where the time goes:
time: 257 us; the launch traced here: 256 us
  waiting for transfers between devices  134 us (52%)
  matrix products  46.8 us (18%)
  starting transfers between devices  20.8 us (8%)
  blocking collectives  19.1 us (7%)
  between operations  13.4 us (5%)
  other arithmetic  13.2 us (5%)
  local copies, waits for them, and re-layouts  8.96 us (3%)
    all_to_all x1, waiting for transfers between devices, sent_to_all(): lax.all_to_all(jnp.broadcast_to(shard[None], (size, *shard.shape)), axis,...  47.8 us
    reduce_scatter x1, waiting for transfers between devices, per_device(): lax.psum_scatter(terms.astype(jnp.bfloat16), 'tp', scatter_dimension=0, t...  45.4 us
    dot_general x1, matrix products, per_device(): jnp.dot(hidden, lax.all_gather(w_down, 'sp', axis=1, tiled=True), preferr...  22.3 us
    all_gather x1, waiting for transfers between devices, per_device(): lax.all_gather(w_down, 'sp', axis=1, tiled=True)  19.4 us
    all_to_all x1, blocking collectives, per_device(): lax.all_to_all(head_out, 'tp', split_axis=0, concat_axis=1, tiled=True)  19.1 us
    dot_general x2, matrix products, add_rows(): return jnp.dot(whole, piece, preferred_element_type=jnp.float32)  18.7 us
    all_gather x1, waiting for transfers between devices, per_device(): lax.all_gather(out_weight, 'tp', axis=0, tiled=True)  16.7 us
    ppermute x5, starting transfers between devices, shifted(): return lax.ppermute(shard, axis, pairs)  15.7 us
  transfers between devices with their start and end apart: 10, of which 5 were waited for; matrix products, arithmetic and copies ran while one was open for 17% of the time, Pallas kernels for 0%

commit v1 on v0

--- a/solution.py
+++ b/solution.py
@@ -5,6 +5,27 @@
 
 HEAD_DIM = 64
 WINDOW = 128
+
+
+def gather_around(shard, axis, dim):
+    count, place, extent = (lax.axis_size(axis), lax.axis_index(axis), shard.shape[dim])
+    upward = [(i, (i + 1) % count) for i in range(count)]
+    downward = [(i, (i - 1) % count) for i in range(count)]
+    out = jnp.zeros((*shard.shape[:dim], count * extent, *shard.shape[dim + 1 :]), shard.dtype)
+    out = lax.dynamic_update_slice_in_dim(out, shard, place * extent, axis=dim)
+    from_left = from_right = shard
+    halfway = count // 2
+    for hop in range(1, halfway + 1):
+        from_left = lax.ppermute(from_left, axis, upward)
+        out = lax.dynamic_update_slice_in_dim(
+            out, from_left, (place - hop) % count * extent, axis=dim
+        )
+        if hop < count - halfway:
+            from_right = lax.ppermute(from_right, axis, downward)
+            out = lax.dynamic_update_slice_in_dim(
+                out, from_right, (place + hop) % count * extent, axis=dim
+            )
+    return out
 
 
 def shifted(shard, axis, by):
@@ -107,9 +128,7 @@
     head_out = attend(queries, key_ext, value_ext, docs_plus, doc_ext, sinks)
     head_rows = lax.all_to_all(head_out, "tp", split_axis=0, concat_axis=1, tiled=True)
     proj = jnp.dot(
-        head_rows,
-        lax.all_gather(out_weight, "tp", axis=0, tiled=True),
-        preferred_element_type=jnp.float32,
+        head_rows, gather_around(out_weight, "tp", 0), preferred_element_type=jnp.float32
     )
     mid32 = (residual.astype(jnp.float32) + proj).astype(jnp.bfloat16).astype(jnp.float32)
     normed = (

time: 257 us -> 238 us (0.926)
  waiting for transfers between devices: 134 us -> 114 us
  blocking collectives: 19.1 us -> 0 us
  local copies, waits for them, and re-layouts: 8.96 us -> 19.1 us
  starting transfers between devices: 20.8 us -> 29.6 us
    all_gather x1, waiting for transfers between devices: 19.4 us -> 0.01 us  [per_device(): lax.all_gather(w_down, 'sp', axis=1, tiled=True)]
    all_to_all x1 -> x0, blocking collectives: 19.1 us -> none  [per_device(): lax.all_to_all(head_out, 'tp', split_axis=0, concat_axis=1, tiled=True)]
    all_gather x1 -> x0, waiting for transfers between devices: 16.7 us -> none  [per_device(): lax.all_gather(out_weight, 'tp', axis=0, tiled=True)]
    ppermute x0 -> x3, waiting for transfers between devices: none -> 15.8 us  [the longest x2 15.8 us: gather_around(): from_left = lax.ppermute(from_left, axis, upward)]
    dynamic_update_slice x0 -> x4, local copies, waits for them, and re-layouts: none -> 5.47 us  [the longest x1 2.32 us: gather_around(): lax.dynamic_update_slice_in_dim(out, from_right, (place + hop) % count *...]
    all_to_all x0 -> x1, waiting for transfers between devices: none -> 4.01 us  [per_device(): lax.all_to_all(head_out, 'tp', split_axis=0, concat_axis=1, tiled=True)]
    all_to_all x0 -> x1, starting transfers between devices: none -> 3.93 us  [per_device(): lax.all_to_all(head_out, 'tp', split_axis=0, concat_axis=1, tiled=True)]
    all_gather x1, waiting for transfers between devices: 3.88 us -> 0.01 us  [side_by_side(): out, at, done = (lax.all_gather(both, axis, axis=dim, tiled=True), 0, [])]
  transfers between devices with their start and end apart: 10 -> 13, of which waited for: 5 -> 4; matrix products, arithmetic and copies ran while one was open for 17% -> 22% of each run, Pallas kernels for 0% -> 0%
where the time goes in v1:
time: 238 us; the launch traced here: 237 us
  waiting for transfers between devices  114 us (48%)
  matrix products  48.1 us (20%)
  starting transfers between devices  29.6 us (12%)
  local copies, waits for them, and re-layouts  19.1 us (8%)
  between operations  13.5 us (6%)
  other arithmetic  13.3 us (6%)
    reduce_scatter x1, waiting for transfers between devices, per_device(): lax.psum_scatter(terms.astype(jnp.bfloat16), 'tp', scatter_dimension=0, t...  47.2 us
    all_to_all x1, waiting for transfers between devices, sent_to_all(): lax.all_to_all(jnp.broadcast_to(shard[None], (size, *shard.shape)), axis,...  46.9 us
    dot_general x1, matrix products, per_device(): jnp.dot(hidden, lax.all_gather(w_down, 'sp', axis=1, tiled=True), preferr...  22.2 us
    dot_general x2, matrix products, add_rows(): return jnp.dot(whole, piece, preferred_element_type=jnp.float32)  18.7 us
    ppermute x5, starting transfers between devices, shifted(): return lax.ppermute(shard, axis, pairs)  16.9 us
    ppermute x2, waiting for transfers between devices, gather_around(): from_left = lax.ppermute(from_left, axis, upward)  15.8 us
    convert_element_type x2, other arithmetic, convolve(): ext32 = ext_rows.astype(jnp.float32)  6.13 us
    all_to_all x1, starting transfers between devices, sent_to_all(): lax.all_to_all(jnp.broadcast_to(shard[None], (size, *shard.shape)), axis,...  5.02 us
  transfers between devices with their start and end apart: 13, of which 4 were waited for; matrix products, arithmetic and copies ran while one was open for 22% of the time, Pallas kernels for 0%

profile of v1, /device:TPU:1, one launch (start us, length us, event | category | flops | bytes accessed | tf_op | source)
XLA Modules:
  0.0 237.4 jit_solution(12315375384478062412)
XLA Ops:
  6.5 1.9 pad_maximum_fusion
  8.5 2.1 collective-permute-start.3
  12.6 4.4 %collective-permute-start.1 = (s32[128]{0:T(128)S(1)}, s32[128]{0:T(128)S(1)}, u32[]{:S(2)}, u32[]{:S(2)}) collective-permute-start(s32[128]{0:T(128)S(1)} %slice.89), channel_id=1, source_target_pairs={{0,4},{4,8},{8,12},{12,16},{16,20},{20,24},{24,28},{28,32},{32,36}... | collective-permute-start | bytes 1544 | tf_op jit(solution)/shard_map/ppermute | solution.py:34
  17.8 1.9 collective-permute-start.2
  20.4 3.6 %collective-permute-start = (bf16[128,64]{0,1:T(8,128)(2,1)S(1)}, bf16[128,64]{0,1:T(8,128)(2,1)S(1)}, u32[]{:S(2)}, u32[]{:S(2)}) collective-permute-start(bf16[128,64]{0,1:T(8,128)(2,1)S(1)} %slice.87), channel_id=1, source_target_pairs={{0,4},{4,8},{8,12},{12,16},{16,20},{20,24},{24,28},{28,32},{32,36}... | collective-permute-start | bytes 49160 | tf_op jit(solution)/shard_map/ppermute | solution.py:34
  26.7 2.5 %broadcast_in_dim.62 = bf16[1024,2048]{1,0:T(8,128)(2,1)} broadcast(bf16[]{:T(256)} %constant.47.clone.1), dimensions={} | broadcast | bytes 4194306 | tf_op jit(solution)/shard_map/broadcast_in_dim | solution.py:14
  30.3 2.0 reshape.131
  38.8 3.9 %all-to-all-start = ((bf16[4,256,256]{1,2,0:T(8,128)(2,1)}), bf16[4,256,256]{1,2,0:T(8,128)(2,1)S(1)}, u32[]{:S(2)}, u32[]{:S(2)}) async-start(bf16[4,256,256]{1,2,0:T(8,128)(2,1)} %copy.33), calls=%async_computation | async-start | bytes 1048576 | tf_op jit(solution)/shard_map/all_to_all | solution.py:129
  43.7 2.3 constant_dynamic-update-slice_fusion.1
  46.0 15.8 %collective-permute-done.5 = bf16[256,2048]{1,0:T(8,128)(2,1)S(1)} collective-permute-done((bf16[256,2048]{1,0:T(8,128)(2,1)S(1)}, bf16[256,2048]{1,0:T(8,128)(2,1)S(1)}, u32[]{:S(2)}, u32[]{:S(2)}) %collective-permute-start.5) | collective-permute-done | bytes 1048608 | tf_op jit(solution)/shard_map/ppermute | solution.py:19
  62.9 4.0 %all-to-all-done = bf16[4,256,256]{1,2,0:T(8,128)(2,1)S(1)} async-done(((bf16[4,256,256]{1,2,0:T(8,128)(2,1)}), bf16[4,256,256]{1,2,0:T(8,128)(2,1)S(1)}, u32[]{:S(2)}, u32[]{:S(2)}) %all-to-all-start) | async-done | bytes 524320 | tf_op jit(solution)/shard_map/all_to_all | solution.py:129
  67.7 4.1 %fusion.24 = (f32[256]{0:T(256)S(1)}, bf16[256,2048]{1,0:T(8,128)(2,1)S(1)}) fusion(bf16[256,1024]{0,1:T(8,128)(2,1)} %bitcast.77, bf16[1024,2048]{1,0:T(8,128)(2,1)} %constant_dynamic-update-slice_fusion, bf16[256,2048]{1,0:T(8,128)(2,1)} %param.18), kind=kOutput, calls=%fused_computation.35 | convolution fusion | flops 1076887296 | bytes 6816768 | tf_op jit(solution)/shard_map/dot_general | solution.py:130
  72.1 2.5 %broadcast_in_dim.63 = bf16[4,256,2048]{2,1,0:T(8,128)(2,1)} broadcast(bf16[256,2048]{1,0:T(8,128)(2,1)S(1)} %fusion.26), dimensions={1,2} | broadcast | bytes 5242880 | tf_op jit(solution)/shard_map/broadcast_in_dim | solution.py:46
  74.6 5.0 %all-to-all-start.1 = ((bf16[4,256,2048]{2,1,0:T(8,128)(2,1)}), bf16[4,256,2048]{2,1,0:T(8,128)(2,1)}, u32[]{:S(2)}, u32[]{:S(2)}) async-start(bf16[4,256,2048]{2,1,0:T(8,128)(2,1)} %broadcast_in_dim.63), calls=%async_computation.1 | async-start | bytes 8388608 | tf_op jit(solution)/shard_map/all_to_all | solution.py:45
  80.2 46.9 %all-to-all-done.1 = bf16[4,256,2048]{2,1,0:T(8,128)(2,1)} async-done(((bf16[4,256,2048]{2,1,0:T(8,128)(2,1)}), bf16[4,256,2048]{2,1,0:T(8,128)(2,1)}, u32[]{:S(2)}, u32[]{:S(2)}) %all-to-all-start.1) | async-done | bytes 4194336 | tf_op jit(solution)/shard_map/all_to_all | solution.py:45
  127.0 10.3 %fusion.14 = bf16[1024,1408]{1,0:T(8,128)(2,1)S(1)} fusion(bf16[1024,2048]{1,0:T(8,128)(2,1)} %bitcast.13, bf16[2048,2816]{1,0:T(8,128)(2,1)} %all-gather.3.cloned.1.call-done), kind=kOutput, calls=%fused_computation.23 | convolution fusion | flops 5907021824 | bytes 12845056 | tf_op jit(solution)/shard_map/dot_general | solution.py:140
  137.3 5.0 %collective-permute-start.6 = (bf16[2,1408]{1,0:T(2,128)(2,1)S(1)}, bf16[2,1408]{1,0:T(2,128)(2,1)S(1)}, u32[]{:S(2)}, u32[]{:S(2)}) collective-permute-start(bf16[2,1408]{1,0:T(2,128)(2,1)S(1)} %slice.114), channel_id=1, source_target_pairs={{0,4},{4,8},{8,12},{12,16},{16,20},{20,24},{24,28},{28,32},{32,36}... | collective-permute-start | bytes 16904 | tf_op jit(solution)/shard_map/ppermute | solution.py:34
  142.4 8.5 %fusion.17 = bf16[1024,1408]{1,0:T(8,128)(2,1)S(1)} fusion(bf16[1024,2048]{1,0:T(8,128)(2,1)} %bitcast.13, bf16[2048,2816]{1,0:T(8,128)(2,1)S(1)} %copy-done.8), kind=kOutput, calls=%fused_computation.24 | convolution fusion | flops 5907021824 | bytes 12845056 | tf_op jit(solution)/shard_map/dot_general | solution.py:140
  150.9 1.9 collective-permute-start.7
  152.8 3.0 %maximum_convert_fusion = f32[1026,1408]{1,0:T(8,128)} fusion(bf16[1024,1408]{1,0:T(8,128)(2,1)S(1)} %fusion.14, bf16[2,1408]{1,0:T(2,128)(2,1)S(1)} %collective-permute-done.6), kind=kLoop, calls=%fused_computation.31 | loop fusion | flops 5778432 | bytes 8667648 | tf_op jit(solution)/shard_map/convert_element_type | solution.py:100
  155.8 3.1 %maximum_convert_fusion.1 = f32[1026,1408]{1,0:T(8,128)} fusion(bf16[1024,1408]{1,0:T(8,128)(2,1)S(1)} %fusion.17, bf16[2,1408]{1,0:T(2,128)(2,1)S(1)} %collective-permute-done.7), kind=kLoop, calls=%fused_computation.32 | loop fusion | flops 5778432 | bytes 8667648 | tf_op jit(solution)/shard_map/convert_element_type | solution.py:100
  158.9 22.2 %convolution_convert_fusion = bf16[1024,2048]{1,0:T(8,128)(2,1)} fusion(bf16[1408,2048]{0,1:T(8,128)(2,1)} %all-gather.5.cloned.1.call-done, f32[1026,1408]{1,0:T(8,128)} %maximum_convert_fusion.1, f32[1026,1408]{1,0:T(8,128)} %maximum_convert_fusion, f32[1408]{0:T(1024)S(1)} %get-tuple-element.9, f32[1408]{0:T(1024)S(1)} %get-tuple-element.10, ...), kind=kOutput, calls=%fused_computation.25 | convolution fusion | flops 5936513024 | bytes 44600320 | tf_op jit(solution)/shard_map/dot_general | solution.py:152
  181.1 47.2 %reduce-scatter.2.cloned.1.call-done = bf16[256,2048]{1,0:T(8,128)(2,1)} async-done(((bf16[1024,2048]{1,0:T(8,128)(2,1)}), bf16[256,2048]{1,0:T(8,128)(2,1)}) %reduce-scatter.2.cloned.1.call-update) | async-done | bytes 1048592 | tf_op jit(solution)/shard_map/reduce_scatter | solution.py:155
  228.3 2.6 %fusion.27 = bf16[256,2048]{1,0:T(8,128)(2,1)} fusion(bf16[256,2048]{1,0:T(8,128)(2,1)S(1)} %get-tuple-element.18, bf16[256,2048]{1,0:T(8,128)(2,1)} %reduce-scatter.2.cloned.1.call-done), kind=kLoop, calls=%fused_computation.38 | loop fusion | flops 2097152 | bytes 3145728 | tf_op jit(solution)/shard_map/convert_element_type | solution.py:158
  (66 shorter events, 17.2 us)
Async XLA Ops:
  6.5 22.7 %copy-start = (bf16[256,2048]{1,0:T(8,128)(2,1)S(1)}, bf16[256,2048]{1,0:T(8,128)(2,1)}, u32[]{:S(2)}) copy-start(bf16[256,2048]{1,0:T(8,128)(2,1)} %param.19) | copy-start | bytes 3145732
  6.5 120.5 %all-gather.3.cloned.1.call-start = ((), (), s32[]{:S(2)}) async-start(), calls=%async_computation.3 | async-start | bytes 11894784 | tf_op jit(solution)/shard_map/all_gather | solution.py:56
  8.4 150.5 %all-gather.5.cloned.1.call-start = ((), (), s32[]{:S(2)}) async-start(), calls=%async_computation.4 | async-start | bytes 5947392 | tf_op jit(solution)/shard_map/all_gather | solution.py:153
  8.5 27.4 %collective-permute-start.3 = (bf16[256,2048]{1,0:T(8,128)(2,1)}, bf16[256,2048]{1,0:T(8,128)(2,1)S(1)}, u32[]{:S(2)}, u32[]{:S(2)}) collective-permute-start(bf16[256,2048]{1,0:T(8,128)(2,1)} %param.19), channel_id=1, source_target_pairs={{0,1},{1,2},{2,3},{3,0},{4,5},{5,6},{6,7},{7,4},{8,9},{9,10},{10,1... | collective-permute-start | bytes 3145736 | tf_op jit(solution)/shard_map/ppermute | solution.py:19
  10.6 33.1 %collective-permute-start.4 = (bf16[256,2048]{1,0:T(8,128)(2,1)}, bf16[256,2048]{1,0:T(8,128)(2,1)}, u32[]{:S(2)}, u32[]{:S(2)}) collective-permute-start(bf16[256,2048]{1,0:T(8,128)(2,1)} %param.19), channel_id=1, source_target_pairs={{0,3},{1,0},{2,1},{3,2},{4,7},{5,4},{6,5},{7,6},{8,11},{9,8},{10,9... | collective-permute-start | bytes 3145736 | tf_op jit(solution)/shard_map/ppermute | solution.py:24
  12.6 19.7 %collective-permute-start.1 = (s32[128]{0:T(128)S(1)}, s32[128]{0:T(128)S(1)}, u32[]{:S(2)}, u32[]{:S(2)}) collective-permute-start(s32[128]{0:T(128)S(1)} %slice.89), channel_id=1, source_target_pairs={{0,4},{4,8},{8,12},{12,16},{16,20},{20,24},{24,28},{28,32},{32,36}... | collective-permute-start | bytes 1544 | tf_op jit(solution)/shard_map/ppermute | solution.py:34
  17.8 15.0 %collective-permute-start.2 = (bf16[128,64]{0,1:T(8,128)(2,1)S(1)}, bf16[128,64]{0,1:T(8,128)(2,1)S(1)}, u32[]{:S(2)}, u32[]{:S(2)}) collective-permute-start(bf16[128,64]{0,1:T(8,128)(2,1)S(1)} %slice.92), channel_id=1, source_target_pairs={{0,4},{4,8},{8,12},{12,16},{16,20},{20,24},{24,28},{28,32},{32,36}... | collective-permute-start | bytes 49160 | tf_op jit(solution)/shard_map/ppermute | solution.py:34
  20.4 15.4 %collective-permute-start = (bf16[128,64]{0,1:T(8,128)(2,1)S(1)}, bf16[128,64]{0,1:T(8,128)(2,1)S(1)}, u32[]{:S(2)}, u32[]{:S(2)}) collective-permute-start(bf16[128,64]{0,1:T(8,128)(2,1)S(1)} %slice.87), channel_id=1, source_target_pairs={{0,4},{4,8},{8,12},{12,16},{16,20},{20,24},{24,28},{28,32},{32,36}... | collective-permute-start | bytes 49160 | tf_op jit(solution)/shard_map/ppermute | solution.py:34
  25.7 7.1 %copy-start.1 = (bf16[1024,64]{0,1:T(8,128)(2,1)S(1)}, bf16[1024,64]{0,1:T(8,128)(2,1)}, u32[]{:S(2)}) copy-start(bf16[1024,64]{0,1:T(8,128)(2,1)} %param.14) | copy-start | bytes 393220
  30.3 4.4 %copy-start.7 = (f32[4]{0:T(128)S(1)}, f32[4]{0:T(128)}, u32[]{:S(2)}) copy-start(f32[4]{0:T(128)} %param.17) | copy-start | bytes 52
  32.8 3.1 %copy-start.2 = (bf16[1024,64]{0,1:T(8,128)(2,1)S(1)}, bf16[1024,64]{0,1:T(8,128)(2,1)}, u32[]{:S(2)}) copy-start(bf16[1024,64]{0,1:T(8,128)(2,1)} %param.15) | copy-start | bytes 393220
  35.9 25.9 %collective-permute-start.5 = (bf16[256,2048]{1,0:T(8,128)(2,1)S(1)}, bf16[256,2048]{1,0:T(8,128)(2,1)S(1)}, u32[]{:S(2)}, u32[]{:S(2)}) collective-permute-start(bf16[256,2048]{1,0:T(8,128)(2,1)S(1)} %collective-permute-done.3), channel_id=1, source_target_pairs={{0,1},{1,2},{2,3},{3,0},{4,5},{5,6},{6,7},{7,4},{8,9},{9,10},{10,1... | collective-permute-start | bytes 3145736 | tf_op jit(solution)/shard_map/ppermute | solution.py:19
  38.8 28.1 %all-to-all-start = ((bf16[4,256,256]{1,2,0:T(8,128)(2,1)}), bf16[4,256,256]{1,2,0:T(8,128)(2,1)S(1)}, u32[]{:S(2)}, u32[]{:S(2)}) async-start(bf16[4,256,256]{1,2,0:T(8,128)(2,1)} %copy.33), calls=%async_computation | async-start | bytes 1048576 | tf_op jit(solution)/shard_map/all_to_all | solution.py:129
  62.9 8.9 %copy-start.6 = (f32[2048]{0:T(1024)S(1)}, f32[2048]{0:T(1024)}, u32[]{:S(2)}) copy-start(f32[2048]{0:T(1024)} %param.20) | copy-start | bytes 24580
  66.9 0.8 copy-start.3
  74.6 5.3 %copy-start.4 = (f32[3,1408]{1,0:T(4,128)S(1)}, f32[3,1408]{1,0:T(4,128)}, u32[]{:S(2)}) copy-start(f32[3,1408]{1,0:T(4,128)} %param.24) | copy-start | bytes 50692
  74.6 5.3 %copy-start.5 = (f32[3,1408]{1,0:T(4,128)S(1)}, f32[3,1408]{1,0:T(4,128)}, u32[]{:S(2)}) copy-start(f32[3,1408]{1,0:T(4,128)} %param.23) | copy-start | bytes 50692
  74.6 52.4 %all-to-all-start.1 = ((bf16[4,256,2048]{2,1,0:T(8,128)(2,1)}), bf16[4,256,2048]{2,1,0:T(8,128)(2,1)}, u32[]{:S(2)}, u32[]{:S(2)}) async-start(bf16[4,256,2048]{2,1,0:T(8,128)(2,1)} %broadcast_in_dim.63), calls=%async_computation.1 | async-start | bytes 8388608 | tf_op jit(solution)/shard_map/all_to_all | solution.py:45
  79.7 148.7 %reduce-scatter.2.cloned.1.call-start = ((), (), s32[]{:S(2)}) async-start(), calls=%async_computation.5 | async-start | bytes 5242880 | tf_op jit(solution)/shard_map/reduce_scatter | solution.py:155
  127.0 15.3 %copy-start.8 = (bf16[2048,2816]{1,0:T(8,128)(2,1)S(1)}, bf16[2048,2816]{1,0:T(8,128)(2,1)}, u32[]{:S(2)}) copy-start(bf16[2048,2816]{1,0:T(8,128)(2,1)} %all-gather.3.cloned.1.call-done) | copy-start | bytes 34603012
  137.3 15.5 %collective-permute-start.6 = (bf16[2,1408]{1,0:T(2,128)(2,1)S(1)}, bf16[2,1408]{1,0:T(2,128)(2,1)S(1)}, u32[]{:S(2)}, u32[]{:S(2)}) collective-permute-start(bf16[2,1408]{1,0:T(2,128)(2,1)S(1)} %slice.114), channel_id=1, source_target_pairs={{0,4},{4,8},{8,12},{12,16},{16,20},{20,24},{24,28},{28,32},{32,36}... | collective-permute-start | bytes 16904 | tf_op jit(solution)/shard_map/ppermute | solution.py:34
  150.9 5.0 %collective-permute-start.7 = (bf16[2,1408]{1,0:T(2,128)(2,1)S(1)}, bf16[2,1408]{1,0:T(2,128)(2,1)S(1)}, u32[]{:S(2)}, u32[]{:S(2)}) collective-permute-start(bf16[2,1408]{1,0:T(2,128)(2,1)S(1)} %slice.121), channel_id=1, source_target_pairs={{0,4},{4,8},{8,12},{12,16},{16,20},{20,24},{24,28},{28,32},{32,36}... | collective-permute-start | bytes 16904 | tf_op jit(solution)/shard_map/ppermute | solution.py:34
Sparse Core Ops, SparseCore 0:
  9.6 63.9 all-gather.2
  75.8 47.7 all-gather.4
  181.3 47.0 reduce-scatter.1
